TPU v7x, 32 devices: a whole 2x2x4 slice. The times are simulated.
32 devices in a mesh: ep: 8 (over z, y), tp: 4 (over x, core).
Axes of the slice: x: 2, y: 2, z: 4, core: 2. Of those that a mesh axis runs over, the one named last changes fastest.
Arguments:
- mixer_in: bfloat16 [8192, 4096], P('ep', 'tp'), may hold values from -110 to 110
- mixer_gain: float32 [4096], P('tp'), may hold values from 0.1 to 1.9
- pool_weight: bfloat16 [4, 1024, 1024], P('tp'), may hold values from -0.1875 to 0.1875
- pool_scale: float32 [4096], P('tp'), may hold values from 0.1 to 1.9
- moe_in: bfloat16 [2048, 4096], P('ep'), may hold values from -6 to 6
- moe_gain: float32 [4096], replicated, may hold values from 0.1 to 1.9
- route_expert: int32 [2048, 2], P('ep'), may hold values from 0 to 7, as said below
- route_weight: float32 [2048, 2], P('ep'), may hold values from 0.1 to 1
- gate_weight: bfloat16 [8, 4096, 1024], P('ep', None, 'tp'), may hold values from -0.09375 to 0.09375
- up_weight: bfloat16 [8, 4096, 1024], P('ep', None, 'tp'), may hold values from -0.09375 to 0.09375
- down_weight: bfloat16 [8, 1024, 4096], P('ep', 'tp'), may hold values from -0.1875 to 0.1875
Outputs:
- mixer_out: bfloat16 [8192, 4096], P('ep', 'tp')
- moe_out: bfloat16 [2048, 4096], P('ep', 'tp')
Inputs may be any that keep to these rules, and one draw needn't show every extreme that they name: `route_expert`: both experts of a row are different and lie in one group: the group of an expert is its number divided by 2, rounded down. Among the rows of one index of ep no expert is named more than 96 times; in every draw the experts of some group are each named exactly 96 times by the rows of every index of ep.
All inputs are finite; a program needn't handle non-finite values.
Results may differ from a plain program's by a relative error of at most 0.0071.
Values may be sent and summed in bfloat16 or wider, within the bound.
A program may use at most 128 MiB of HBM per device.

v0:
```python
import functools

import jax
import jax.numpy as jnp
from jax import lax
from jax.experimental import pallas as pl
from jax.experimental.pallas import tpu as pltpu
from jax.sharding import PartitionSpec as P

D = 4096
WINDOW_MAX = 16


EPS = 1e-06


def passed_along(value, axis, steps):
    count = lax.axis_size(axis)
    first, last = (max(0, -steps), min(count, count - steps))
    return lax.ppermute(value, axis, [(source, source + steps) for source in range(first, last)])


GROUPS = 4
MESH = pl.DeviceIdType.MESH


def expert_kernel(
    cap,
    out_ref,
    wrow_ref,
    gate_hbm,
    up_hbm,
    down_hbm,
    mixer_hbm,
    gain_ref,
    pool_hbm,
    scale_ref,
    fin_ref,
    mixed_ref,
    xbuf,
    wbuf,
    wcol,
    w_gate,
    w_up,
    w_down,
    part_out,
    part_in,
    sums,
    first_in,
    second_in,
    local_sem,
    wsend,
    wrecv,
    zsend,
    zrecv,
    csend,
    crecv,
    psend,
    precv,
    fsend,
    frecv,
    feats,
    w_pool,
    squares,
    squares_in,
    factors,
    normed,
    msend,
    mrecv,
):
    ep, tp = lax.axis_index("ep"), lax.axis_index("tp")
    z, y = ep // 2, ep % 2
    x, c = tp // 2, tp % 2
    width = out_ref.shape[1]
    pair = 2 * cap

    def dev(zz, yy, xx, cc):
        return (zz * 2 + yy, xx * 2 + cc)

    core_peer = dev(z, y, x, 1 - c)
    x_peer = dev(z, y, 1 - x, c)
    y_peer = dev(z, 1 - y, x, c)

    loads = [
        pltpu.make_async_copy(gate_hbm, w_gate, local_sem.at[0]),
        pltpu.make_async_copy(up_hbm, w_up, local_sem.at[1]),
        pltpu.make_async_copy(down_hbm, w_down, local_sem.at[2]),
    ]
    mixer_load = pltpu.make_async_copy(mixer_hbm, feats, local_sem.at[5])
    pool_load = pltpu.make_async_copy(pool_hbm, w_pool, local_sem.at[6])
    mixer_load.start()
    for load in loads:
        load.start()
    pool_load.start()

    barrier = pltpu.get_barrier_semaphore()
    cross_peer = dev(z, y, 1 - x, 1 - c)
    peers = [core_peer, x_peer, y_peer, cross_peer]
    for dz in range(GROUPS):
        for other in range(2):
            if dz or other:
                peer = dev(lax.rem(z + dz, GROUPS), lax.rem(y + other, 2), x, c)
                if not (dz == 0 and other == 1):
                    peers.append(peer)
    for peer in peers:
        pl.semaphore_signal(barrier, inc=1, device_id=peer, device_id_type=MESH)
    pl.semaphore_wait(barrier, len(peers))

    def remote(src, dst, send, recv, peer):
        copy = pltpu.make_async_remote_copy(
            src_ref=src,
            dst_ref=dst,
            send_sem=send,
            recv_sem=recv,
            device_id=peer,
            device_id_type=MESH,
        )
        return copy

    def source_rows(zz, yy):
        return pl.ds(pl.multiple_of((zz * 2 + yy) * cap, cap), cap)

    def group_rows(g):
        return pl.ds(pl.multiple_of(g * cap, cap), cap)

    started = []

    def go(copy):
        copy.start()
        started.append(copy)
        return copy

    zcopies = [None]
    for dz in range(1, GROUPS):
        g = lax.rem(z + dz, GROUPS)
        zcopies.append(
            go(
                remote(
                    out_ref.at[group_rows(g), :],
                    xbuf.at[tp, source_rows(z, y), :],
                    zsend.at[dz],
                    zrecv.at[dz],
                    dev(g, y, x, c),
                )
            )
        )
    keep = pltpu.make_async_copy(
        out_ref.at[group_rows(z), :], xbuf.at[tp, source_rows(z, y), :], local_sem.at[3]
    )
    keep.start()
    keep_w = pltpu.make_async_copy(wrow_ref.at[z], wbuf.at[ep], local_sem.at[4])
    keep_w.start()
    wcopies = []
    for dz in range(GROUPS):
        for other in range(2):
            if dz or other:
                g = lax.rem(z + dz, GROUPS)
                wcopies.append(
                    go(
                        remote(
                            wrow_ref.at[g],
                            wbuf.at[ep],
                            wsend.at[dz * 2 + other],
                            wrecv.at[dz * 2 + other],
                            dev(g, lax.rem(y + other, 2), x, c),
                        )
                    )
                )

    xq = (1 - x) * 2 + c
    piece = {}

    half = width // 2

    def share(name, index, k, quarter, yy, peer, part=None):
        rows = source_rows(lax.rem(z + GROUPS - k, GROUPS), yy)
        cols = slice(None) if part is None else pl.ds(part * half, half)
        ref = xbuf.at[quarter, rows, cols]
        slot = index * GROUPS + k
        piece[name, k] = go(remote(ref, ref, csend.at[slot], crecv.at[slot], peer))

    def own(k):
        if k:
            zcopies[k].wait_recv()
        else:
            keep.wait()
        share("x", 0, k, tp, y, x_peer)
        share("y", 1, k, tp, y, y_peer)
        share("c", 2, k, tp, y, core_peer)

    def relay(k):
        piece["x", k].wait_recv()
        share("d0", 3, k, xq, y, y_peer, 0)
        share("xc", 4, k, xq, y, core_peer)
        piece["y", k].wait_recv()
        share("d1", 7, k, tp, 1 - y, x_peer, 1)
        share("yc", 5, k, tp, 1 - y, core_peer)

    def diagonal(k):
        piece["d0", k].wait_recv()
        piece["d1", k].wait_recv()
        share("dc", 6, k, xq, 1 - y, core_peer)

    def complete(k):
        for name in ("c", "xc", "yc", "dc"):
            piece[name, k].wait_recv()

    def chunk_rows(k):
        return pl.ds(pl.multiple_of(lax.rem(z + GROUPS - k, GROUPS) * pair, pair), pair)

    def columns(xx, cc):
        return pl.ds(pl.multiple_of((xx * 2 + cc) * width, width), width)

    hidden = {}
    away = {}

    def expand(k):
        rows = chunk_rows(k)
        gate = jnp.zeros((pair, w_gate.shape[1]), jnp.float32)
        upper = gate
        for q in range(xbuf.shape[0]):
            block = xbuf[q, rows, :]
            gate += jnp.dot(
                block, w_gate[q * width : (q + 1) * width, :], preferred_element_type=jnp.float32
            )
            upper += jnp.dot(
                block, w_up[q * width : (q + 1) * width, :], preferred_element_type=jnp.float32
            )
        scale = wcol[rows, :]
        scale = jnp.concatenate([scale] * (w_gate.shape[1] // scale.shape[1]), axis=1)
        value = (gate / (1.0 + jnp.exp(-gate))) * upper * scale
        hidden[k] = value.astype(jnp.bfloat16)
        for xx in range(2):
            part_out[k, xx] = jnp.dot(
                hidden[k], w_down[:, columns(xx, 1 - c)], preferred_element_type=jnp.float32
            ).astype(jnp.bfloat16)
            slot = k * 2 + xx
            away[k, xx] = go(
                remote(
                    part_out.at[k, xx], part_in.at[k, xx], psend.at[slot], precv.at[slot], core_peer
                )
            )

    hop = {}

    def first_hop(k):
        for xx in range(2):
            mine = jnp.dot(
                hidden[k], w_down[:, columns(xx, c)], preferred_element_type=jnp.float32
            )
            away[k, xx].wait_recv()
            sums[k, xx] = (mine + part_in[k, xx].astype(jnp.float32)).astype(jnp.bfloat16)
        hop[k, 0] = go(
            remote(
                sums.at[k, 1 - x, :, 0:half],
                first_in.at[k, 0],
                fsend.at[k * 6],
                frecv.at[k * 6],
                x_peer,
            )
        )
        for xx in range(2):
            hop[k, 1 + xx] = go(
                remote(
                    sums.at[k, xx, group_rows(1 - y), half:width],
                    first_in.at[k, 1, xx * cap : (xx + 1) * cap, :],
                    fsend.at[k * 6 + 1 + xx],
                    frecv.at[k * 6 + 1 + xx],
                    y_peer,
                )
            )

    def second_hop(k):
        hop[k, 0].wait_recv()
        total = sums[k, x, :, 0:half].astype(jnp.float32) + first_in[k, 0].astype(jnp.float32)
        sums[k, x, :, 0:half] = total.astype(jnp.bfloat16)
        hop[k, 3] = go(
            remote(
                sums.at[k, x, group_rows(1 - y), 0:half],
                second_in.at[k, 0],
                fsend.at[k * 6 + 3],
                frecv.at[k * 6 + 3],
                y_peer,
            )
        )
        for xx in range(2):
            hop[k, 1 + xx].wait_recv()
            total = sums[k, xx, group_rows(y), half:width].astype(jnp.float32) + first_in[
                k, 1, xx * cap : (xx + 1) * cap, :
            ].astype(jnp.float32)
            sums[k, xx, group_rows(y), half:width] = total.astype(jnp.bfloat16)
        hop[k, 4] = go(
            remote(
                sums.at[k, 1 - x, group_rows(y), half:width],
                second_in.at[k, 1],
                fsend.at[k * 6 + 4],
                frecv.at[k * 6 + 4],
                x_peer,
            )
        )

    home = {}

    def homeward(k):
        for part in range(2):
            cols = slice(part * half, (part + 1) * half)
            hop[k, 3 + part].wait_recv()
            total = sums[k, x, group_rows(y), cols].astype(jnp.float32) + second_in[
                k, part
            ].astype(jnp.float32)
            if k == 0:
                fin_ref[group_rows(z), cols] = total.astype(jnp.bfloat16)
            else:
                sums[k, x, group_rows(y), cols] = total.astype(jnp.bfloat16)
        if k:
            home[k] = go(
                remote(
                    sums.at[k, x, group_rows(y), :],
                    fin_ref.at[group_rows(z), :],
                    fsend.at[k * 6 + 5],
                    frecv.at[k * 6 + 5],
                    dev(lax.rem(z + GROUPS - k, GROUPS), y, x, c),
                )
            )

    rows, channels = feats.shape
    tiles = rows // 128
    reach = WINDOW_MAX

    def tile_rows(i, start=0, count=128):
        return pl.ds(pl.multiple_of(i * 128 + start, 16), count)

    mixer_copies = []

    def square_sums():
        mixer_load.wait()

        @pl.loop(0, tiles)
        def _(i):
            total = jnp.zeros((128, 128), jnp.float32)
            for q in range(channels // 128):
                value = feats[tile_rows(i), q * 128 : (q + 1) * 128].astype(jnp.float32)
                total += value * value
            squares[pl.ds(i, 1), :] = jnp.sum(total.T, axis=0, keepdims=True)

        for index, peer in enumerate((core_peer, x_peer, cross_peer)):
            mixer_copies.append(
                go(
                    remote(
                        squares, squares_in.at[index], msend.at[index], mrecv.at[index], peer
                    )
                )
            )

    def normalize():
        for copy in mixer_copies:
            copy.wait_recv()
        total = squares[...] + squares_in[0] + (squares_in[1] + squares_in[2])
        factors[...] = lax.rsqrt(total / D + EPS)

        @pl.loop(0, tiles)
        def _(i):
            factor = jnp.broadcast_to(factors[pl.ds(i, 1), :], (128, 128)).T
            for q in range(channels // 128):
                cols = slice(q * 128, (q + 1) * 128)
                value = feats[tile_rows(i), cols].astype(jnp.float32) * factor * gain_ref[:, cols]
                normed[tile_rows(i, reach), cols] = value.astype(jnp.bfloat16)

        following = lax.rem(ep + 1, 2 * GROUPS)
        mixer_copies.append(
            go(
                remote(
                    normed.at[rows : rows + reach, :],
                    normed.at[0:reach, :],
                    msend.at[3],
                    mrecv.at[3],
                    (following, tp),
                )
            )
        )

    def halo():
        mixer_copies[3].wait_recv()
        edge = normed[0:reach, :]
        normed[0:reach, :] = jnp.where(ep == 0, jnp.zeros_like(edge), edge)
        pool_load.wait()

    def pool(first, last):
        span = jnp.where(tp == 0, 2, jnp.where(tp == 1, 4, jnp.where(tp == 2, 8, 16)))

        @pl.loop(first, last)
        def _(i):
            position = ep * rows + i * 128 + lax.broadcasted_iota(jnp.int32, (128, 256), 0)
            share_of = 1.0 / jnp.minimum(position + 1, span).astype(jnp.float32)
            for q in range(channels // 256):
                cols = slice(q * 256, (q + 1) * 256)
                value = normed[tile_rows(i, 0, 128 + reach), cols].astype(jnp.float32)
                two = value + pltpu.roll(value, 1, 0)
                four = two + pltpu.roll(two, 2, 0)
                eight = four + pltpu.roll(four, 4, 0)
                sixteen = eight + pltpu.roll(eight, 8, 0)
                window = jnp.where(
                    tp == 0, two, jnp.where(tp == 1, four, jnp.where(tp == 2, eight, sixteen))
                )
                pooled = window[reach:] * share_of - value[reach:]
                feats[tile_rows(i), cols] = pooled.astype(jnp.bfloat16)
            projected = jnp.dot(
                feats[tile_rows(i), :], w_pool[...], preferred_element_type=jnp.float32
            )
            mixed_ref[tile_rows(i), :] = (projected * scale_ref[...]).astype(jnp.bfloat16)

    own(0)
    square_sums()
    own(1)
    relay(0)
    normalize()
    own(2)
    relay(1)
    halo()
    pool(0, tiles // 4)
    diagonal(0)
    own(3)
    pool(tiles // 4, tiles // 2)
    keep_w.wait()
    for copy in wcopies:
        copy.wait_recv()
    for source in range(wbuf.shape[0]):
        line = jnp.where(y == 0, wbuf[source, 0:1, :], wbuf[source, 1:2, :])
        wcol[source * cap : (source + 1) * cap, :] = jnp.broadcast_to(line, (128, 128)).T[:cap]
    for load in loads:
        load.wait()
    complete(0)
    expand(0)
    relay(2)
    diagonal(1)
    first_hop(0)
    relay(3)
    complete(1)
    expand(1)
    diagonal(2)
    first_hop(1)
    complete(2)
    expand(2)
    diagonal(3)
    first_hop(2)
    second_hop(0)
    complete(3)
    expand(3)
    first_hop(3)
    second_hop(1)
    homeward(1)
    second_hop(2)
    second_hop(3)
    homeward(2)
    pool(tiles // 2, 5 * tiles // 8)
    homeward(3)
    homeward(0)
    pool(5 * tiles // 8, tiles)
    for k in range(1, GROUPS):
        home[k].wait_recv()
    for copy in started:
        copy.wait_send()


def paired_step(
    mixer_in,
    mixer_gain,
    pool_weight,
    pool_scale,
    moe_in,
    moe_gain,
    route_expert,
    route_weight,
    gate_weight,
    up_weight,
    down_weight,
):
    tokens = moe_in.shape[0]
    n_ep, n_tp = lax.axis_size("ep"), lax.axis_size("tp")
    cap = 3 * tokens // n_ep
    width = moe_in.shape[1] // n_tp
    units = gate_weight.shape[2]
    tp = lax.axis_index("tp")
    slots = GROUPS * cap
    group = route_expert[:, 0] // 2
    lanes = jnp.arange(GROUPS, dtype=jnp.int32)
    member = group[:, None] == lanes[None, :]
    order = jnp.arange(tokens, dtype=jnp.int32)
    before = (order[:, None] > order[None, :]).astype(jnp.bfloat16)
    ahead = jnp.dot(before, member.astype(jnp.bfloat16), preferred_element_type=jnp.float32)
    rank = jnp.sum(jnp.where(member, ahead, 0.0), axis=1).astype(jnp.int32)
    slot = group * cap + rank
    select = (jnp.arange(slots, dtype=jnp.int32)[:, None] == slot[None, :]).astype(jnp.bfloat16)
    feats = moe_in.astype(jnp.float32)
    factor = lax.rsqrt(jnp.mean(feats * feats, axis=1, keepdims=True) + EPS)
    mine = lax.dynamic_slice_in_dim(moe_in, tp * width, width, 1).astype(jnp.float32)
    gain = lax.dynamic_slice_in_dim(moe_gain, tp * width, width, 0)
    normed = (mine * factor * gain).astype(jnp.bfloat16)
    outgoing = jnp.dot(select, normed, preferred_element_type=jnp.float32).astype(jnp.bfloat16)
    lane = jnp.arange(128, dtype=jnp.int32)
    wide = (rank[:, None] == lane[None, :]).astype(jnp.float32)
    by_expert = jnp.sum(
        jnp.where(
            (route_expert % 2)[:, :, None] == jnp.arange(8, dtype=jnp.int32)[None, None, :],
            route_weight[:, :, None],
            0.0,
        ),
        axis=1,
    )
    spread = (member[:, :, None] * by_expert[:, None, :]).reshape(tokens, GROUPS * 8)
    wrow = jnp.dot(
        spread.T, wide, precision=lax.Precision.HIGHEST, preferred_element_type=jnp.float32
    ).reshape(GROUPS, 8, 128)
    vmem = pl.BlockSpec(memory_space=pltpu.VMEM)
    hbm = pl.BlockSpec(memory_space=pl.ANY)
    dma = pltpu.SemaphoreType.DMA
    model = moe_in.shape[1]
    rows, channels = mixer_in.shape
    fin, mixer_out = pl.pallas_call(
        functools.partial(expert_kernel, cap),
        out_shape=(
            jax.ShapeDtypeStruct((slots, width), jnp.bfloat16),
            jax.ShapeDtypeStruct((rows, channels), jnp.bfloat16),
        ),
        in_specs=[vmem, vmem, hbm, hbm, hbm, hbm, vmem, hbm, vmem],
        out_specs=(vmem, vmem),
        scratch_shapes=[
            pltpu.VMEM((n_tp, n_ep * cap, width), jnp.bfloat16),
            pltpu.VMEM((n_ep, 8, 128), jnp.float32),
            pltpu.VMEM((n_ep * cap, 128), jnp.float32),
            pltpu.VMEM((model, units), jnp.bfloat16),
            pltpu.VMEM((model, units), jnp.bfloat16),
            pltpu.VMEM((units, model), jnp.bfloat16),
            pltpu.VMEM((GROUPS, 2, 2 * cap, width), jnp.bfloat16),
            pltpu.VMEM((GROUPS, 2, 2 * cap, width), jnp.bfloat16),
            pltpu.VMEM((GROUPS, 2, 2 * cap, width), jnp.bfloat16),
            pltpu.VMEM((GROUPS, 2, 2 * cap, width // 2), jnp.bfloat16),
            pltpu.VMEM((GROUPS, 2, cap, width // 2), jnp.bfloat16),
            dma((7,)),
            dma((8,)),
            dma((8,)),
            dma((4,)),
            dma((4,)),
            dma((32,)),
            dma((32,)),
            dma((8,)),
            dma((8,)),
            dma((24,)),
            dma((24,)),
            pltpu.VMEM((rows, channels), jnp.bfloat16),
            pltpu.VMEM(pool_weight.shape[1:], jnp.bfloat16),
            pltpu.VMEM((rows // 128, 128), jnp.float32),
            pltpu.VMEM((3, rows // 128, 128), jnp.float32),
            pltpu.VMEM((rows // 128, 128), jnp.float32),
            pltpu.VMEM((rows + WINDOW_MAX, channels), jnp.bfloat16),
            dma((4,)),
            dma((4,)),
        ],
        compiler_params=pltpu.CompilerParams(
            collective_id=0, has_side_effects=True, vmem_limit_bytes=56 * 1024 * 1024
        ),
    )(
        outgoing,
        wrow,
        gate_weight[0],
        up_weight[0],
        down_weight[0],
        mixer_in,
        mixer_gain[None, :],
        pool_weight[0],
        pool_scale[None, :],
    )
    moe_out = lax.dot_general(
        select, fin, (((0,), (0,)), ((), ())), preferred_element_type=jnp.float32
    ).astype(jnp.bfloat16)
    return (mixer_out, moe_out)


def any_experts(
    moe_in, moe_gain, route_expert, route_weight, gate_weight, up_weight, down_weight
):
    tokens = moe_in.shape[0]
    feats_b = moe_in.astype(jnp.float32)
    normed_b = (
        feats_b * lax.rsqrt(jnp.mean(feats_b * feats_b, axis=1, keepdims=True) + EPS) * moe_gain
    ).astype(jnp.bfloat16)
    experts = gate_weight.shape[0] * lax.axis_size("ep")
    slots = 3 * tokens // experts
    flat = route_expert.reshape(-1)
    onehot = (flat[:, None] == jnp.arange(experts, dtype=jnp.int32)[None, :]).astype(jnp.int32)
    earlier = jnp.cumsum(onehot, axis=0) - onehot
    slot_index = flat * slots + jnp.sum(earlier * onehot, axis=1)
    owner = jnp.arange(2 * tokens, dtype=jnp.int32) // 2
    source = jnp.full((experts * slots,), tokens, jnp.int32).at[slot_index].set(owner)
    padded_b = jnp.concatenate([normed_b, jnp.zeros((1, D), jnp.bfloat16)], axis=0)
    outgoing = jnp.take(padded_b, source, axis=0).reshape(experts, slots, D)
    w_gate = gate_weight[0]
    w_up = up_weight[0]
    share = slots // lax.axis_size("tp")
    mine = lax.dynamic_slice_in_dim(outgoing, lax.axis_index("tp") * share, share, 1)
    arrived = lax.all_to_all(mine, "ep", split_axis=0, concat_axis=0, tiled=True)
    expand_arrived = lax.all_gather(arrived, "tp", axis=1, tiled=True)
    gate = jnp.einsum("nkd,df->nkf", expand_arrived, w_gate, preferred_element_type=jnp.float32)
    upper = jnp.einsum("nkd,df->nkf", expand_arrived, w_up, preferred_element_type=jnp.float32)
    hidden = (jax.nn.silu(gate) * upper).astype(jnp.bfloat16)
    flat_hidden = hidden.reshape(-1, hidden.shape[2])
    w_down = down_weight[0]
    columns = D // lax.axis_size("tp")
    summed = lax.psum_scatter(
        lax.dot_general(
            w_down, flat_hidden, (((0,), (1,)), ((), ())), preferred_element_type=jnp.float32
        ),
        "tp",
        scatter_dimension=0,
        tiled=True,
    ).astype(jnp.bfloat16)
    back = lax.all_to_all(
        summed.reshape(columns, -1, slots), "ep", split_axis=1, concat_axis=1, tiled=True
    )
    picked = jnp.take(back.reshape(columns, experts * slots), slot_index, axis=1)
    weighted = picked.astype(jnp.float32).reshape(columns, tokens, 2) * route_weight[None, :, :]
    moe_out = jnp.sum(weighted, axis=2).T.astype(jnp.bfloat16)
    return moe_out


def general_step(
    mixer_in,
    mixer_gain,
    pool_weight,
    pool_scale,
    moe_in,
    moe_gain,
    route_expert,
    route_weight,
    gate_weight,
    up_weight,
    down_weight,
):
    rows = mixer_in.shape[0]
    feats = mixer_in.astype(jnp.float32)
    squares = lax.psum(jnp.sum(feats * feats, axis=1), "tp")
    normed_a = (feats * lax.rsqrt(squares[:, None] / D + EPS) * mixer_gain).astype(jnp.bfloat16)
    reach = WINDOW_MAX - 1
    before = passed_along(normed_a[rows - reach :], "ep", 1)
    extended = jnp.concatenate([before, normed_a], axis=0).astype(jnp.float32)
    running = jnp.zeros((rows, normed_a.shape[1]), jnp.float32)
    totals = []
    for offset in range(WINDOW_MAX):
        running = running + lax.slice_in_dim(
            extended, reach - offset, reach - offset + rows, axis=0
        )
        if offset > 0 and offset + 1 & offset == 0:
            totals.append(running)
    group = lax.axis_index("tp")
    window_sum = lax.dynamic_index_in_dim(jnp.stack(totals), group, 0, keepdims=False)
    span = jnp.left_shift(jnp.int32(2), group)
    position = lax.axis_index("ep") * rows + jnp.arange(rows, dtype=jnp.int32)
    count = jnp.minimum(position + 1, span).astype(jnp.float32)[:, None]
    pooled = (window_sum / count - extended[reach:]).astype(jnp.bfloat16)
    mixer_out = (
        jnp.dot(pooled, pool_weight[0], preferred_element_type=jnp.float32) * pool_scale
    ).astype(jnp.bfloat16)
    moe_out = any_experts(
        moe_in, moe_gain, route_expert, route_weight, gate_weight, up_weight, down_weight
    )
    return (mixer_out, moe_out)


def solution(mesh):
    paired = mesh.shape["ep"] == 2 * GROUPS and mesh.shape["tp"] == 4
    return jax.shard_map(
        paired_step if paired else general_step,
        mesh=mesh,
        in_specs=(
            P("ep", "tp"),
            P("tp"),
            P("tp", None, None),
            P("tp"),
            P("ep", None),
            P(),
            P("ep", None),
            P("ep", None),
            P("ep", None, "tp"),
            P("ep", None, "tp"),
            P("ep", "tp", None),
        ),
        out_specs=(P("ep", "tp"), P("ep", "tp")),
        check_vma=False,
    )
```

profile of v0, /device:TPU:0, one launch (start us, length us, event | category | flops | bytes accessed | tf_op | source)
XLA Modules:
  0.0 95.2 jit_solution(16192861686082265667)
XLA Ops:
  0.6 0.0 copy-start
  0.6 0.0 copy-start.1
  0.7 0.0 dynamic-slice-start
  0.7 0.7 and_select_fusion.1
  1.4 0.2 fusion
  1.6 2.1 %multiply_reduce_fusion = f32[256]{0:T(256)S(1)} fusion(bf16[256,4096]{1,0:T(8,128)(2,1)} %param.15), kind=kLoop, calls=%fused_computation | loop fusion | flops 3145472 | bytes 2098176 | tf_op jit(solution)/shard_map/reduce_sum | solution.py:495
  3.7 0.0 dynamic-slice-done
  3.7 2.4 %convolution_convert_fusion.out_ref = bf16[384,1024]{1,0:T(8,128)(2,1)} fusion(f32[1024]{0:T(1024)S(1)} %dynamic-slice-done, f32[256]{0:T(256)S(1)} %add_rsqrt_fusion, bf16[256,4096]{1,0:T(8,128)(2,1)} %param.15, s32[]{:T(128)} %select_n.34, s32[256]{0:T(256)S(1)} %multiply_add_fusion), kind=kOutput, calls=%fused_computation.1 | convolution fusion | flops 202866688 | bytes 1317376 | tf_op jit(solution)/shard_map/dot_general | solution.py:499
  6.2 0.0 copy-done
  6.2 0.0 copy-done.1
  6.2 0.9 fusion.7.wrow_ref
  7.1 82.7 %shard_map.122 = (bf16[384,1024]{1,0:T(8,128)(2,1)}, bf16[1024,1024]{1,0:T(8,128)(2,1)}) custom-call(bf16[384,1024]{1,0:T(8,128)(2,1)} %convolution_convert_fusion.out_ref, f32[4,8,128]{2,1,0:T(8,128)} %fusion.7.wrow_ref, bf16[4096,256]{1,0:T(8,128)(2,1)} %bitcast.19, bf16[4096,256]{1,0:T(8,128)(2,1)} %bitcast.20, bf16[256,4096]{1,0:T(8,128)(2,1)} %bitcast.21, ...), custom_call_target="tpu_custom_call" | custom-call | tf_op jit(solution)/shard_map/pallas_call | solution.py:519
  89.7 2.4 %convolution_convert_fusion.1 = bf16[256,1024]{1,0:T(8,128)(2,1)} fusion(bf16[384,1024]{1,0:T(8,128)(2,1)} %get-tuple-element.5, s32[256]{0:T(256)S(1)} %multiply_add_fusion), kind=kOutput, calls=%fused_computation.2 | convolution fusion | flops 201687040 | bytes 1311744 | tf_op jit(solution)/shard_map/dot_general | solution.py:573
  92.2 3.1 %copy.16 = bf16[1024,1024]{1,0:T(8,128)(2,1)} copy(bf16[1024,1024]{1,0:T(8,128)(2,1)} %get-tuple-element.10) | data formatting | bytes 4194304
  (6 shorter events, 0.0 us)
Async XLA Ops:
  0.6 5.5 %copy-start = (s32[256,2]{0,1:T(2,128)S(1)}, s32[256,2]{0,1:T(2,128)}, u32[]{:S(2)}) copy-start(s32[256,2]{0,1:T(2,128)} %param.17) | copy-start | bytes 6148
  0.6 5.5 %copy-start.1 = (f32[256,2]{0,1:T(2,128)S(1)}, f32[256,2]{0,1:T(2,128)}, u32[]{:S(2)}) copy-start(f32[256,2]{0,1:T(2,128)} %param.18) | copy-start | bytes 6148
  0.7 3.1 %dynamic-slice-start = ((f32[4096]{0:T(1024)}, s32[]{:T(128)}), f32[1024]{0:T(1024)S(1)}, s32[]{:S(2)}) async-start(f32[4096]{0:T(1024)} %param.16, s32[]{:T(128)} %select_n.34), calls=%async_computation | async-start | bytes 8704 | tf_op jit(solution)/shard_map/dynamic_slice | solution.py:497
where the time goes:
time: 95.6 us; the launch traced here: 95.2 us
  Pallas kernels  82.7 us (87%)
  matrix products  5.9 us (6%)
  local copies, waits for them, and re-layouts  3.09 us (3%)
  other arithmetic  2.86 us (3%)
    pallas_call x1, Pallas kernels, paired_step(): pl.pallas_call(functools.partial(expert_kernel, cap), out_shape=(jax.Shap...  82.7 us
    unnamed x5, local copies, waits for them, and re-layouts  3.09 us
    dot_general x1, matrix products, paired_step(): jnp.dot(select, normed, preferred_element_type=jnp.float32)  2.43 us
    dot_general x1, matrix products, paired_step(): lax.dot_general(select, fin, (((0,), (0,)), ((), ())), preferred_element_...  2.42 us
    reduce_sum x1, other arithmetic, paired_step(): factor = lax.rsqrt(jnp.mean(feats * feats, axis=1, keepdims=True) + EPS)  2.09 us

commit v1 on v0

v1 whole, which is shorter than its diff:
```python
import functools

import jax
import jax.numpy as jnp
from jax import lax
from jax.experimental import pallas as pl
from jax.experimental.pallas import tpu as pltpu
from jax.sharding import PartitionSpec as P

D = 4096
WINDOW_MAX = 16


EPS = 1e-06


def passed_along(value, axis, steps):
    count = lax.axis_size(axis)
    first, last = (max(0, -steps), min(count, count - steps))
    return lax.ppermute(value, axis, [(source, source + steps) for source in range(first, last)])


GROUPS = 4
MESH = pl.DeviceIdType.MESH


def expert_kernel(
    cap,
    parts,
    moe_hbm,
    moe_gain_ref,
    routes_ref,
    shares_ref,
    gate_hbm,
    up_hbm,
    down_hbm,
    mixer_hbm,
    gain_ref,
    pool_hbm,
    scale_ref,
    moe_ref,
    mixed_ref,
    tokens_in,
    row_factor,
    scaled,
    outgoing,
    slot_column,
    unpermuted,
    xbuf,
    wrow,
    wbuf,
    wcol,
    w_gate,
    w_up,
    w_down,
    hidden,
    sums,
    first_x,
    first_y,
    second_in,
    fin,
    local_sem,
    send_sem,
    recv_sem,
    feats,
    w_pool,
    squares,
    squares_in,
    factors,
    normed,
):
    ep, tp = lax.axis_index("ep"), lax.axis_index("tp")
    z, y = ep // 2, ep % 2
    x, c = tp // 2, tp % 2
    tokens, model = tokens_in.shape
    width = xbuf.shape[3]
    units = w_gate.shape[1]
    half = width // 2
    part = cap // parts
    pair = 2 * part
    mine, theirs = slice(0, part), slice(part, pair)
    chunks = range(GROUPS * parts)
    eighth = width // 8
    direct = tuple(share * eighth for share in (4, 4, 0, 0, 0, 0, 8, 8))

    def dev(zz, yy, xx, cc):
        return (zz * 2 + yy, xx * 2 + cc)

    planes = [z, z + 1 - 2 * (z % 2), lax.rem(z + 2, GROUPS), GROUPS - 1 - z]
    core_peer = dev(z, y, x, 1 - c)
    x_peer = dev(z, y, 1 - x, c)
    y_peer = dev(z, 1 - y, x, c)
    cross_peer = dev(z, y, 1 - x, 1 - c)
    xq = (1 - x) * 2 + c

    def columns(quarter, count=None, offset=0):
        start = pl.multiple_of(quarter * width + offset, 128)
        return pl.ds(start, width if count is None else count)

    block = tokens // 8
    token_loads = [
        pltpu.make_async_copy(
            moe_hbm.at[b * block : (b + 1) * block],
            tokens_in.at[b * block : (b + 1) * block],
            local_sem.at[b],
        )
        for b in range(8)
    ]
    mixer_load = pltpu.make_async_copy(mixer_hbm, feats, local_sem.at[8])
    pool_load = pltpu.make_async_copy(pool_hbm, w_pool, local_sem.at[9])
    loads = [
        pltpu.make_async_copy(gate_hbm, w_gate, local_sem.at[10]),
        pltpu.make_async_copy(up_hbm, w_up, local_sem.at[11]),
    ]
    down_rows = pl.ds(pl.multiple_of(c * units, units), units)
    for xx in range(2):
        loads.append(
            pltpu.make_async_copy(
                down_hbm.at[:, columns(xx * 2 + c)],
                w_down.at[xx, down_rows, :],
                local_sem.at[12 + xx],
            )
        )
    for load in token_loads:
        load.start()

    barrier = pltpu.get_barrier_semaphore()
    peers = [core_peer, x_peer, y_peer, cross_peer]
    for other in range(2):
        for k in range(1, GROUPS):
            peers.append(dev(planes[k], lax.rem(y + other, 2), x, c))
    for peer in peers:
        pl.semaphore_signal(barrier, inc=1, device_id=peer, device_id_type=MESH)

    started = []

    def go(src, dst, peer):
        index = len(started)
        copy = pltpu.make_async_remote_copy(
            src_ref=src,
            dst_ref=dst,
            send_sem=send_sem.at[index],
            recv_sem=recv_sem.at[index],
            device_id=peer,
            device_id_type=MESH,
        )
        copy.start()
        started.append(copy)
        return copy

    routes = routes_ref[...]
    group = jnp.right_shift(routes[0:1, :], 1)
    lane_group = lax.broadcasted_iota(jnp.int32, (8, tokens), 0)
    member = lane_group == group
    earlier = lax.broadcasted_iota(jnp.int32, (tokens, tokens), 0) < lax.broadcasted_iota(
        jnp.int32, (tokens, tokens), 1
    )
    ahead = jnp.dot(
        member.astype(jnp.bfloat16), earlier.astype(jnp.bfloat16), preferred_element_type=jnp.float32
    )
    rank = jnp.sum(jnp.where(member, ahead, 0.0), axis=0, keepdims=True).astype(jnp.int32)

    def picks(k, count):
        place = lax.broadcasted_iota(jnp.int32, (count, tokens), 0)
        return (place == rank) & (group == planes[k])

    parity = jnp.bitwise_and(routes, 1)
    shares = shares_ref[...]
    by_expert = jnp.sum(
        jnp.concatenate(
            [
                jnp.where(lane_group == parity[r : r + 1, :], shares[r : r + 1, :], 0.0)[None]
                for r in range(2)
            ],
            axis=0,
        ),
        axis=0,
    )
    slot = (group * cap + rank).astype(jnp.float32)
    for b in range(tokens // 128):
        row = slot[:, b * 128 : (b + 1) * 128]
        slot_column[b * 128 : (b + 1) * 128, :] = jnp.broadcast_to(row, (128, 128)).T

    for k in range(GROUPS):
        wrow[k] = lax.dot_general(
            by_expert,
            picks(k, 128).astype(jnp.float32),
            (((1,), (1,)), ((), ())),
            precision=lax.Precision.HIGHEST,
            preferred_element_type=jnp.float32,
        )
    wbuf[0] = wrow[0]

    for b in range(8):
        token_loads[b].wait()
        rows = slice(b * block, (b + 1) * block)
        total = jnp.zeros((block, 128), jnp.float32)
        for q in range(model // 128):
            value = tokens_in[rows, q * 128 : (q + 1) * 128].astype(jnp.float32)
            total += value * value
        mean = jnp.sum(total, axis=1, keepdims=True) / D
        row_factor[rows, :] = jnp.broadcast_to(lax.rsqrt(mean + EPS), (block, 128))
    for load in (mixer_load, *loads, pool_load):
        load.start()

    def scale_quarter(quarter):
        for j in range(width // 128):
            cols = columns(quarter, 128, j * 128)
            value = tokens_in[:, cols].astype(jnp.float32) * row_factor[...]
            scaled[:, j * 128 : (j + 1) * 128] = (value * moe_gain_ref[:, cols]).astype(
                jnp.bfloat16
            )

    flushed = [0]

    def flush(recent):
        last = max(flushed[0], len(started) - recent)
        for copy in started[flushed[0] : last]:
            copy.wait_send()
        flushed[0] = last

    def own_rows(quarter):
        return [xbuf.at[quarter, h, mine] for h in range(parts)]

    def pick_rows(quarter, groups, targets):
        scale_quarter(quarter)
        choose = jnp.concatenate(
            [picks(k, cap).astype(jnp.float32) for k in groups], axis=0
        ).astype(jnp.bfloat16)
        for j in range(width // 256):
            cols = slice(j * 256, (j + 1) * 256)
            picked = jnp.dot(
                choose, scaled[:, cols], preferred_element_type=jnp.float32
            ).astype(jnp.bfloat16)
            start = 0
            for target in targets:
                target[:, cols] = picked[start : start + target.shape[0]]
                start += target.shape[0]

    zcopies = {}
    piece = {}

    def depart(k, across):
        g = k // parts
        index = g if g > 1 else across
        rows = slice(k % parts * part, (k % parts + 1) * part)
        zcopies[k, across] = go(
            outgoing.at[index, rows],
            xbuf.at[xq if across else tp, k, mine],
            dev(planes[g], y, x, c),
        )

    def share(name, k, quarter, source, target, peer, start=0, stop=None):
        stop = width if stop is None else stop
        if start < stop:
            cols = pl.ds(start, stop - start)
            piece[name, k] = go(
                xbuf.at[quarter, k, source, cols], xbuf.at[quarter, k, target, cols], peer
            )

    pick_rows(tp, (1, 2, 3, 0), [outgoing.at[0], outgoing.at[2], outgoing.at[3]] + own_rows(tp))
    pl.semaphore_wait(barrier, len(peers))
    wcopies = []
    for k in range(GROUPS):
        for r in range(2):
            if k or r:
                peer = dev(planes[k], lax.rem(y + r, 2), x, c)
                wcopies.append(go(wrow.at[k], wbuf.at[k * 2 + r], peer))
    depart(5, 0)
    depart(2, 0)
    depart(3, 0)
    for k in range(parts):
        share("y", k, tp, mine, theirs, y_peer)
    pick_rows(xq, (1, 0), [outgoing.at[1]] + own_rows(xq))
    depart(2, 1)
    depart(6, 0)
    depart(4, 0)
    depart(7, 0)
    depart(3, 1)
    for k in range(parts):
        share("d0", k, xq, mine, theirs, y_peer, 0, direct[k])
    down_copies = []
    for xx in range(2):
        down_copies.append(
            go(down_hbm.at[:, columns(xx * 2 + 1 - c)], w_down.at[xx, down_rows, :], core_peer)
        )
    for quarter in (x * 2 + 1 - c, (1 - x) * 2 + 1 - c):
        pick_rows(quarter, (0,), own_rows(quarter))

    def arrive(k):
        zcopies[k, 0].wait_recv()
        share("y", k, tp, mine, theirs, y_peer)
        if k // parts > 1:
            share("x", k, tp, mine, mine, x_peer)
        share("c", k, tp, mine, mine, core_peer)

    def across(k):
        if k // parts == 1:
            zcopies[k, 1].wait_recv()
        else:
            piece["x", k].wait_recv()
        share("d0", k, xq, mine, theirs, y_peer, 0, direct[k])
        share("xc", k, xq, mine, mine, core_peer)

    def relay(k):
        piece["y", k].wait_recv()
        share("d1", k, tp, theirs, theirs, x_peer, direct[k])
        share("yc", k, tp, theirs, theirs, core_peer)

    def diagonal(k):
        for name in ("d0", "d1"):
            if (name, k) in piece:
                piece[name, k].wait_recv()
        share("dc", k, xq, theirs, theirs, core_peer)

    def complete(k):
        for name in ("c", "xc", "yc", "dc"):
            if (name, k) in piece:
                piece[name, k].wait_recv()

    hidden_away = {}

    def weights_ready():
        for copy in wcopies:
            copy.wait_recv()
        for source in range(wbuf.shape[0]):
            line = jnp.where(y == 0, wbuf[source, 0:1, :], wbuf[source, 1:2, :])
            wcol[source * cap : (source + 1) * cap, :] = jnp.broadcast_to(line, (128, 128)).T[:cap]
        for load in loads:
            load.wait()
        for copy in down_copies:
            copy.wait_recv()

    def expand(k):
        complete(k)
        gate = jnp.zeros((pair, units), jnp.float32)
        upper = gate
        for q in range(xbuf.shape[0]):
            rows = xbuf[q, k]
            gate += jnp.dot(
                rows, w_gate[q * width : (q + 1) * width, :], preferred_element_type=jnp.float32
            )
            upper += jnp.dot(
                rows, w_up[q * width : (q + 1) * width, :], preferred_element_type=jnp.float32
            )
        first = k // parts * 2 * cap + k % parts * part
        scale = jnp.concatenate(
            [wcol[first : first + part, :], wcol[first + cap : first + cap + part, :]], axis=0
        )
        scale = jnp.concatenate([scale] * (units // scale.shape[1]), axis=1)
        value = (gate / (1.0 + jnp.exp(-gate))) * upper * scale
        hidden[c, k] = value.astype(jnp.bfloat16)
        hidden_away[k] = go(hidden.at[c, k], hidden.at[c, k], core_peer)

    hop = {}

    def project(k):
        hidden_away[k].wait_recv()
        for xx in range(2):
            for j in range(2):
                cols = slice(j * half, (j + 1) * half)
                total = jnp.dot(
                    hidden[0, k], w_down[xx, 0:units, cols], preferred_element_type=jnp.float32
                ) + jnp.dot(
                    hidden[1, k], w_down[xx, units:, cols], preferred_element_type=jnp.float32
                )
                sums[k, xx, :, cols] = total.astype(jnp.bfloat16)
        hop[k, 0] = go(sums.at[k, 1 - x, :, 0:half], first_x.at[k], x_peer)
        hop[k, 1] = go(sums.at[k, :, theirs, half:width], first_y.at[k], y_peer)

    def second_x(k):
        hop[k, 0].wait_recv()
        total = sums[k, x, :, 0:half].astype(jnp.float32) + first_x[k].astype(jnp.float32)
        sums[k, x, :, 0:half] = total.astype(jnp.bfloat16)
        hop[k, 3] = go(sums.at[k, x, theirs, 0:half], second_in.at[k, 0], y_peer)

    def second_y(k):
        hop[k, 1].wait_recv()
        for xx in range(2):
            total = sums[k, xx, mine, half:width].astype(jnp.float32) + first_y[k, xx].astype(
                jnp.float32
            )
            sums[k, xx, mine, half:width] = total.astype(jnp.bfloat16)
        hop[k, 4] = go(sums.at[k, 1 - x, mine, half:width], second_in.at[k, 1], x_peer)

    home = {}

    def homeward(k):
        for piece_index in range(2):
            cols = slice(piece_index * half, (piece_index + 1) * half)
            hop[k, 3 + piece_index].wait_recv()
            total = sums[k, x, mine, cols].astype(jnp.float32) + second_in[
                k, piece_index
            ].astype(jnp.float32)
            if k < parts:
                fin[k, :, cols] = total.astype(jnp.bfloat16)
            else:
                sums[k, x, mine, cols] = total.astype(jnp.bfloat16)
        if k >= parts:
            home[k] = go(sums.at[k, x, mine, :], fin.at[k], dev(planes[k // parts], y, x, c))

    settled = []

    def settle(k):
        if k >= parts:
            home[k].wait_recv()
        first = planes[k // parts] * cap + k % parts * part
        place = lax.broadcasted_iota(jnp.int32, (tokens, part), 1) + first
        choose = (slot_column[:, 0:part].astype(jnp.int32) == place).astype(jnp.float32)
        choose = choose.astype(jnp.bfloat16)
        settled.append(k)
        for j in range(width // 256):
            cols = slice(j * 256, (j + 1) * 256)
            value = jnp.dot(choose, fin[k, :, cols], preferred_element_type=jnp.float32)
            if len(settled) > 1:
                value += unpermuted[:, cols]
            if len(settled) == len(chunks):
                moe_ref[:, cols] = value.astype(jnp.bfloat16)
            else:
                unpermuted[:, cols] = value

    rows, channels = feats.shape
    tiles = rows // 128
    reach = WINDOW_MAX

    def tile_rows(i, start=0, count=128):
        return pl.ds(pl.multiple_of(i * 128 + start, 16), count)

    mixer_copies = []

    def square_sums():
        mixer_load.wait()

        @pl.loop(0, tiles)
        def _(i):
            total = jnp.zeros((128, 128), jnp.float32)
            for q in range(channels // 128):
                value = feats[tile_rows(i), q * 128 : (q + 1) * 128].astype(jnp.float32)
                total += value * value
            squares[pl.ds(i, 1), :] = jnp.sum(total.T, axis=0, keepdims=True)

        for index, peer in enumerate((core_peer, x_peer, cross_peer)):
            mixer_copies.append(
                go(squares, squares_in.at[index], peer)
            )

    def normalize():
        for copy in mixer_copies:
            copy.wait_recv()
        total = squares[...] + squares_in[0] + (squares_in[1] + squares_in[2])
        factors[...] = lax.rsqrt(total / D + EPS)

        @pl.loop(0, tiles)
        def _(i):
            factor = jnp.broadcast_to(factors[pl.ds(i, 1), :], (128, 128)).T
            for q in range(channels // 128):
                cols = slice(q * 128, (q + 1) * 128)
                value = feats[tile_rows(i), cols].astype(jnp.float32) * factor * gain_ref[:, cols]
                normed[tile_rows(i, reach), cols] = value.astype(jnp.bfloat16)

        following = lax.rem(ep + 1, 2 * GROUPS)
        mixer_copies.append(
            go(normed.at[rows : rows + reach, :], normed.at[0:reach, :], (following, tp))
        )

    def halo():
        mixer_copies[3].wait_recv()
        edge = normed[0:reach, :]
        normed[0:reach, :] = jnp.where(ep == 0, jnp.zeros_like(edge), edge)
        pool_load.wait()

    def pool(first, last):
        span = jnp.where(tp == 0, 2, jnp.where(tp == 1, 4, jnp.where(tp == 2, 8, 16)))

        @pl.loop(first, last)
        def _(i):
            position = ep * rows + i * 128 + lax.broadcasted_iota(jnp.int32, (128, 256), 0)
            share_of = 1.0 / jnp.minimum(position + 1, span).astype(jnp.float32)
            for q in range(channels // 256):
                cols = slice(q * 256, (q + 1) * 256)
                value = normed[tile_rows(i, 0, 128 + reach), cols].astype(jnp.float32)
                two = value + pltpu.roll(value, 1, 0)
                four = two + pltpu.roll(two, 2, 0)
                eight = four + pltpu.roll(four, 4, 0)
                sixteen = eight + pltpu.roll(eight, 8, 0)
                window = jnp.where(
                    tp == 0, two, jnp.where(tp == 1, four, jnp.where(tp == 2, eight, sixteen))
                )
                pooled = window[reach:] * share_of - value[reach:]
                feats[tile_rows(i), cols] = pooled.astype(jnp.bfloat16)
            projected = jnp.dot(
                feats[tile_rows(i), :], w_pool[...], preferred_element_type=jnp.float32
            )
            mixed_ref[tile_rows(i), :] = (projected * scale_ref[...]).astype(jnp.bfloat16)

    relay(0)
    arrive(2)
    diagonal(0)
    relay(1)
    weights_ready()
    arrive(5)
    relay(2)
    expand(0)
    relay(5)
    arrive(3)
    project(0)
    across(2)
    diagonal(1)
    diagonal(2)
    arrive(4)
    square_sums()
    arrive(6)
    expand(2)
    across(5)
    across(3)
    project(2)
    arrive(7)
    relay(4)
    across(6)
    diagonal(5)
    relay(3)
    expand(5)
    second_x(2)
    normalize()
    second_x(0)
    across(4)
    across(7)
    relay(6)
    diagonal(4)
    relay(7)
    second_y(0)
    second_y(2)
    project(5)
    halo()
    diagonal(6)
    expand(4)
    pool(0, 1)
    flush(24)
    homeward(0)
    expand(1)
    project(4)
    diagonal(7)
    expand(7)
    second_x(5)
    second_y(5)
    expand(6)
    homeward(2)
    project(7)
    second_x(4)
    diagonal(3)
    pool(1, 2)
    flush(24)
    second_y(4)
    project(6)
    expand(3)
    homeward(5)
    pool(2, 3)
    flush(24)
    pool(3, 4)
    flush(24)
    homeward(4)
    project(3)
    second_y(7)
    second_x(7)
    second_y(6)
    second_x(6)
    second_x(3)
    second_y(3)
    project(1)
    pool(4, 5)
    flush(24)
    homeward(6)
    pool(5, 6)
    flush(24)
    flush(16)
    settle(0)
    homeward(7)
    pool(6, 7)
    flush(24)
    flush(16)
    settle(4)
    homeward(3)
    flush(16)
    settle(2)
    second_x(1)
    second_y(1)
    pool(7, 8)
    flush(24)
    flush(16)
    settle(6)
    homeward(1)
    flush(16)
    settle(5)
    flush(16)
    settle(1)
    flush(16)
    settle(3)
    flush(16)
    settle(7)
    flush(0)


def deliver(moe_in_ref, mixed_in_ref, moe_hbm, mixer_hbm, sem):
    copies = []
    for source, target, count in ((mixed_in_ref, mixer_hbm, 16), (moe_in_ref, moe_hbm, 4)):
        rows = source.shape[0] // count
        for i in range(count):
            at = slice(i * rows, (i + 1) * rows)
            copies.append(
                pltpu.make_async_copy(source.at[at], target.at[at], sem.at[len(copies)])
            )
    for copy in copies:
        copy.start()
    for copy in copies:
        copy.wait()


def paired_step(
    mixer_in,
    mixer_gain,
    pool_weight,
    pool_scale,
    moe_in,
    moe_gain,
    route_expert,
    route_weight,
    gate_weight,
    up_weight,
    down_weight,
):
    tokens, model = moe_in.shape
    n_ep, n_tp = lax.axis_size("ep"), lax.axis_size("tp")
    cap = 3 * tokens // n_ep
    width = model // n_tp
    units = gate_weight.shape[2]
    vmem = pl.BlockSpec(memory_space=pltpu.VMEM)
    hbm = pl.BlockSpec(memory_space=pl.ANY)
    dma = pltpu.SemaphoreType.DMA
    rows, channels = mixer_in.shape
    copies = 150
    parts = 2
    chunks, part = GROUPS * parts, cap // parts
    moe_shape = (tokens, width)
    mixer_shape = (rows, channels)
    moe_out, mixed = pl.pallas_call(
        functools.partial(expert_kernel, cap, parts),
        out_shape=(
            pltpu.VMEM(moe_shape, jnp.bfloat16),
            pltpu.VMEM(mixer_shape, jnp.bfloat16),
        ),
        in_specs=[hbm, vmem, vmem, vmem, hbm, hbm, hbm, hbm, vmem, hbm, vmem],
        out_specs=(vmem, vmem),
        scratch_shapes=[
            pltpu.VMEM((tokens, model), jnp.bfloat16),
            pltpu.VMEM((tokens, 128), jnp.float32),
            pltpu.VMEM((tokens, width), jnp.bfloat16),
            pltpu.VMEM((GROUPS, cap, width), jnp.bfloat16),
            pltpu.VMEM((tokens, 128), jnp.float32),
            pltpu.VMEM((tokens, width), jnp.float32),
            pltpu.VMEM((n_tp, chunks, 2 * part, width), jnp.bfloat16),
            pltpu.VMEM((GROUPS, 8, 128), jnp.float32),
            pltpu.VMEM((n_ep, 8, 128), jnp.float32),
            pltpu.VMEM((n_ep * cap, 128), jnp.float32),
            pltpu.VMEM((model, units), jnp.bfloat16),
            pltpu.VMEM((model, units), jnp.bfloat16),
            pltpu.VMEM((2, 2 * units, width), jnp.bfloat16),
            pltpu.VMEM((2, chunks, 2 * part, units), jnp.bfloat16),
            pltpu.VMEM((chunks, 2, 2 * part, width), jnp.bfloat16),
            pltpu.VMEM((chunks, 2 * part, width // 2), jnp.bfloat16),
            pltpu.VMEM((chunks, 2, part, width // 2), jnp.bfloat16),
            pltpu.VMEM((chunks, 2, part, width // 2), jnp.bfloat16),
            pltpu.VMEM((chunks, part, width), jnp.bfloat16),
            dma((14,)),
            dma((copies,)),
            dma((copies,)),
            pltpu.VMEM((rows, channels), jnp.bfloat16),
            pltpu.VMEM(pool_weight.shape[1:], jnp.bfloat16),
            pltpu.VMEM((rows // 128, 128), jnp.float32),
            pltpu.VMEM((3, rows // 128, 128), jnp.float32),
            pltpu.VMEM((rows // 128, 128), jnp.float32),
            pltpu.VMEM((rows + WINDOW_MAX, channels), jnp.bfloat16),
        ],
        compiler_params=pltpu.CompilerParams(
            collective_id=0, has_side_effects=True, vmem_limit_bytes=56 * 1024 * 1024
        ),
    )(
        moe_in,
        moe_gain[None, :],
        route_expert.T,
        route_weight.T,
        gate_weight[0],
        up_weight[0],
        down_weight[0],
        mixer_in,
        mixer_gain[None, :],
        pool_weight[0],
        pool_scale[None, :],
    )
    moe_out, mixer_out = pl.pallas_call(
        deliver,
        out_shape=(
            jax.ShapeDtypeStruct(moe_shape, jnp.bfloat16),
            jax.ShapeDtypeStruct(mixer_shape, jnp.bfloat16),
        ),
        in_specs=[vmem, vmem],
        out_specs=(hbm, hbm),
        scratch_shapes=[dma((20,))],
    )(
        pltpu.with_memory_space_constraint(moe_out, pltpu.VMEM),
        pltpu.with_memory_space_constraint(mixed, pltpu.VMEM),
    )
    return (mixer_out, moe_out)


def any_experts(
    moe_in, moe_gain, route_expert, route_weight, gate_weight, up_weight, down_weight
):
    tokens = moe_in.shape[0]
    feats_b = moe_in.astype(jnp.float32)
    normed_b = (
        feats_b * lax.rsqrt(jnp.mean(feats_b * feats_b, axis=1, keepdims=True) + EPS) * moe_gain
    ).astype(jnp.bfloat16)
    experts = gate_weight.shape[0] * lax.axis_size("ep")
    slots = 3 * tokens // experts
    flat = route_expert.reshape(-1)
    onehot = (flat[:, None] == jnp.arange(experts, dtype=jnp.int32)[None, :]).astype(jnp.int32)
    earlier = jnp.cumsum(onehot, axis=0) - onehot
    slot_index = flat * slots + jnp.sum(earlier * onehot, axis=1)
    owner = jnp.arange(2 * tokens, dtype=jnp.int32) // 2
    source = jnp.full((experts * slots,), tokens, jnp.int32).at[slot_index].set(owner)
    padded_b = jnp.concatenate([normed_b, jnp.zeros((1, D), jnp.bfloat16)], axis=0)
    outgoing = jnp.take(padded_b, source, axis=0).reshape(experts, slots, D)
    w_gate = gate_weight[0]
    w_up = up_weight[0]
    share = slots // lax.axis_size("tp")
    mine = lax.dynamic_slice_in_dim(outgoing, lax.axis_index("tp") * share, share, 1)
    arrived = lax.all_to_all(mine, "ep", split_axis=0, concat_axis=0, tiled=True)
    expand_arrived = lax.all_gather(arrived, "tp", axis=1, tiled=True)
    gate = jnp.einsum("nkd,df->nkf", expand_arrived, w_gate, preferred_element_type=jnp.float32)
    upper = jnp.einsum("nkd,df->nkf", expand_arrived, w_up, preferred_element_type=jnp.float32)
    hidden = (jax.nn.silu(gate) * upper).astype(jnp.bfloat16)
    flat_hidden = hidden.reshape(-1, hidden.shape[2])
    w_down = down_weight[0]
    columns = D // lax.axis_size("tp")
    summed = lax.psum_scatter(
        lax.dot_general(
            w_down, flat_hidden, (((0,), (1,)), ((), ())), preferred_element_type=jnp.float32
        ),
        "tp",
        scatter_dimension=0,
        tiled=True,
    ).astype(jnp.bfloat16)
    back = lax.all_to_all(
        summed.reshape(columns, -1, slots), "ep", split_axis=1, concat_axis=1, tiled=True
    )
    picked = jnp.take(back.reshape(columns, experts * slots), slot_index, axis=1)
    weighted = picked.astype(jnp.float32).reshape(columns, tokens, 2) * route_weight[None, :, :]
    moe_out = jnp.sum(weighted, axis=2).T.astype(jnp.bfloat16)
    return moe_out


def general_step(
    mixer_in,
    mixer_gain,
    pool_weight,
    pool_scale,
    moe_in,
    moe_gain,
    route_expert,
    route_weight,
    gate_weight,
    up_weight,
    down_weight,
):
    rows = mixer_in.shape[0]
    feats = mixer_in.astype(jnp.float32)
    squares = lax.psum(jnp.sum(feats * feats, axis=1), "tp")
    normed_a = (feats * lax.rsqrt(squares[:, None] / D + EPS) * mixer_gain).astype(jnp.bfloat16)
    reach = WINDOW_MAX - 1
    before = passed_along(normed_a[rows - reach :], "ep", 1)
    extended = jnp.concatenate([before, normed_a], axis=0).astype(jnp.float32)
    running = jnp.zeros((rows, normed_a.shape[1]), jnp.float32)
    totals = []
    for offset in range(WINDOW_MAX):
        running = running + lax.slice_in_dim(
            extended, reach - offset, reach - offset + rows, axis=0
        )
        if offset > 0 and offset + 1 & offset == 0:
            totals.append(running)
    group = lax.axis_index("tp")
    window_sum = lax.dynamic_index_in_dim(jnp.stack(totals), group, 0, keepdims=False)
    span = jnp.left_shift(jnp.int32(2), group)
    position = lax.axis_index("ep") * rows + jnp.arange(rows, dtype=jnp.int32)
    count = jnp.minimum(position + 1, span).astype(jnp.float32)[:, None]
    pooled = (window_sum / count - extended[reach:]).astype(jnp.bfloat16)
    mixer_out = (
        jnp.dot(pooled, pool_weight[0], preferred_element_type=jnp.float32) * pool_scale
    ).astype(jnp.bfloat16)
    moe_out = any_experts(
        moe_in, moe_gain, route_expert, route_weight, gate_weight, up_weight, down_weight
    )
    return (mixer_out, moe_out)


def solution(mesh):
    paired = mesh.shape["ep"] == 2 * GROUPS and mesh.shape["tp"] == 4
    return jax.shard_map(
        paired_step if paired else general_step,
        mesh=mesh,
        in_specs=(
            P("ep", "tp"),
            P("tp"),
            P("tp", None, None),
            P("tp"),
            P("ep", None),
            P(),
            P("ep", None),
            P("ep", None),
            P("ep", None, "tp"),
            P("ep", None, "tp"),
            P("ep", "tp", None),
        ),
        out_specs=(P("ep", "tp"), P("ep", "tp")),
        check_vma=False,
    )
```

time: 95.6 us -> 71.5 us (0.75)
  Pallas kernels: 82.7 us -> 70.4 us
  matrix products: 5.9 us -> 0 us
  local copies, waits for them, and re-layouts: 3.09 us -> 0 us
  other arithmetic: 2.86 us -> 0 us
    pallas_call x1 -> x2, Pallas kernels: 82.7 us -> 70.4 us  [the longest x1 68.8 us: paired_step(): pl.pallas_call(functools.partial(expert_kernel, cap, parts), out_shape=(p...]
    dot_general x4 -> x0, matrix products: 5.9 us -> none  [the longest x1 2.43 us: paired_step(): jnp.dot(select, normed, preferred_element_type=jnp.float32)]
    unnamed x5 -> x0, local copies, waits for them, and re-layouts: 3.09 us -> none
    reduce_sum x2 -> x0, other arithmetic: 2.09 us -> none  [the longest x1 2.09 us: paired_step(): factor = lax.rsqrt(jnp.mean(feats * feats, axis=1, keepdims=True) + EPS)]
where the time goes in v1:
time: 71.5 us; the launch traced here: 71.2 us
  Pallas kernels  70.4 us (98%)
  between operations  0.8 us (1%)
    pallas_call x1, Pallas kernels, paired_step(): pl.pallas_call(functools.partial(expert_kernel, cap, parts), out_shape=(p...  68.8 us
    pallas_call x1, Pallas kernels, paired_step(): pl.pallas_call(deliver, out_shape=(jax.ShapeDtypeStruct(moe_shape, jnp.bf...  1.65 us

profile of v1, /device:TPU:0, one launch (start us, length us, event | category | flops | bytes accessed | tf_op | source)
XLA Modules:
  0.0 71.2 jit_solution(16783564762699623729)
XLA Ops:
  0.6 68.8 %shard_map.122 = (bf16[256,1024]{1,0:T(8,128)(2,1)S(1)}, bf16[1024,1024]{1,0:T(8,128)(2,1)S(1)}) custom-call(bf16[256,4096]{1,0:T(8,128)(2,1)} %moe_hbm.1, f32[1,4096]{1,0:T(1,128)} %bitcast.13, s32[2,256]{1,0:T(2,128)} %bitcast.16, f32[2,256]{1,0:T(2,128)} %bitcast.17, bf16[4096,256]{1,0:T(8,128)(2,1)} %bitcast.9, bf16[4096,256]{1,0:T(8,128)(2,1)} %bitcast.10, ...), custom_call_target="tpu_custom_call" | custom-call | tf_op jit(solution)/shard_map/pallas_call | solution.py:645
  69.4 1.6 %shard_map.123 = (bf16[256,1024]{1,0:T(8,128)(2,1)}, bf16[1024,1024]{1,0:T(8,128)(2,1)}) custom-call(bf16[256,1024]{1,0:T(8,128)(2,1)S(1)} %get-tuple-element.6.moe_in_ref, bf16[1024,1024]{1,0:T(8,128)(2,1)S(1)} %get-tuple-element.7.mixed_in_ref), custom_call_target="tpu_custom_call" | custom-call | tf_op jit(solution)/shard_map/pallas_call | solution.py:699

commit v2 on v1

--- a/solution.py
+++ b/solution.py
@@ -27,19 +27,25 @@
 def expert_kernel(
     cap,
     parts,
+    spare,
     moe_hbm,
-    moe_gain_ref,
-    routes_ref,
-    shares_ref,
+    moe_gain_hbm,
+    routes_hbm,
+    shares_hbm,
     gate_hbm,
     up_hbm,
     down_hbm,
     mixer_hbm,
-    gain_ref,
+    gain_hbm,
     pool_hbm,
-    scale_ref,
+    scale_hbm,
     moe_ref,
     mixed_ref,
+    moe_gain_ref,
+    routes_ref,
+    shares_ref,
+    gain_ref,
+    scale_ref,
     tokens_in,
     row_factor,
     scaled,
@@ -50,6 +56,7 @@
     wrow,
     wbuf,
     wcol,
+    fcol,
     w_gate,
     w_up,
     w_down,
@@ -97,15 +104,29 @@
         start = pl.multiple_of(quarter * width + offset, 128)
         return pl.ds(start, width if count is None else count)
 
-    block = tokens // 8
-    token_loads = [
-        pltpu.make_async_copy(
-            moe_hbm.at[b * block : (b + 1) * block],
-            tokens_in.at[b * block : (b + 1) * block],
-            local_sem.at[b],
+    quarters = (tp, xq, x * 2 + 1 - c, (1 - x) * 2 + 1 - c)
+    rows_half = tokens // 2
+    small_loads = [
+        pltpu.make_async_copy(source, target, local_sem.at[16 + i])
+        for i, (source, target) in enumerate(
+            (
+                (routes_hbm, routes_ref),
+                (shares_hbm, shares_ref),
+                (moe_gain_hbm, moe_gain_ref),
+                (gain_hbm, gain_ref),
+                (scale_hbm, scale_ref),
+            )
         )
-        for b in range(8)
     ]
+    token_loads = []
+    for i, quarter in enumerate(quarters):
+        for b in range(2):
+            at = (slice(b * rows_half, (b + 1) * rows_half), columns(quarter))
+            token_loads.append(
+                pltpu.make_async_copy(
+                    moe_hbm.at[at], tokens_in.at[at], local_sem.at[i * 2 + b]
+                )
+            )
     mixer_load = pltpu.make_async_copy(mixer_hbm, feats, local_sem.at[8])
     pool_load = pltpu.make_async_copy(pool_hbm, w_pool, local_sem.at[9])
     loads = [
@@ -121,7 +142,7 @@
                 local_sem.at[12 + xx],
             )
         )
-    for load in token_loads:
+    for load in small_loads[:3] + token_loads + small_loads[3:]:
         load.start()
 
     barrier = pltpu.get_barrier_semaphore()
@@ -134,12 +155,23 @@
 
     started = []
 
-    def go(src, dst, peer):
+    ring = []
+    kept = []
+
+    def go(src, dst, peer, keep=False):
         index = len(started)
+        if keep:
+            send = spare + len(kept)
+            kept.append(index)
+        else:
+            send = len(ring) % spare
+            if len(ring) >= spare:
+                started[ring[-spare]].wait_send()
+            ring.append(index)
         copy = pltpu.make_async_remote_copy(
             src_ref=src,
             dst_ref=dst,
-            send_sem=send_sem.at[index],
+            send_sem=send_sem.at[send],
             recv_sem=recv_sem.at[index],
             device_id=peer,
             device_id_type=MESH,
@@ -148,6 +180,8 @@
         started.append(copy)
         return copy
 
+    for load in small_loads[:3]:
+        load.wait()
     routes = routes_ref[...]
     group = jnp.right_shift(routes[0:1, :], 1)
     lane_group = lax.broadcasted_iota(jnp.int32, (8, tokens), 0)
@@ -181,43 +215,45 @@
         row = slot[:, b * 128 : (b + 1) * 128]
         slot_column[b * 128 : (b + 1) * 128, :] = jnp.broadcast_to(row, (128, 128)).T
 
-    for k in range(GROUPS):
-        wrow[k] = lax.dot_general(
-            by_expert,
-            picks(k, 128).astype(jnp.float32),
-            (((1,), (1,)), ((), ())),
-            precision=lax.Precision.HIGHEST,
-            preferred_element_type=jnp.float32,
+    def send_lines():
+        for b in range(8):
+            rows = slice(b * tokens // 8, (b + 1) * tokens // 8)
+            total = jnp.zeros((tokens // 8, 128), jnp.float32)
+            for q in range(model // 128):
+                value = tokens_in[rows, q * 128 : (q + 1) * 128].astype(jnp.float32)
+                total += value * value
+            mean = jnp.sum(total, axis=1, keepdims=True) / D
+            row_factor[rows, :] = jnp.broadcast_to(lax.rsqrt(mean + EPS), (tokens // 8, 128))
+        factor = jnp.concatenate(
+            [row_factor[b * 128 : (b + 1) * 128, :].T[0:8, :] for b in range(tokens // 128)], axis=1
         )
-    wbuf[0] = wrow[0]
-
-    for b in range(8):
-        token_loads[b].wait()
-        rows = slice(b * block, (b + 1) * block)
-        total = jnp.zeros((block, 128), jnp.float32)
-        for q in range(model // 128):
-            value = tokens_in[rows, q * 128 : (q + 1) * 128].astype(jnp.float32)
-            total += value * value
-        mean = jnp.sum(total, axis=1, keepdims=True) / D
-        row_factor[rows, :] = jnp.broadcast_to(lax.rsqrt(mean + EPS), (block, 128))
+        lines = jnp.where(lane_group == 2, factor, by_expert)
+        copies = []
+        for k in range(GROUPS):
+            wrow[k] = lax.dot_general(
+                lines,
+                picks(k, 128).astype(jnp.float32),
+                (((1,), (1,)), ((), ())),
+                precision=lax.Precision.HIGHEST,
+                preferred_element_type=jnp.float32,
+            )
+            for r in range(2):
+                if k or r:
+                    peer = dev(planes[k], lax.rem(y + r, 2), x, c)
+                    copies.append(go(wrow.at[k], wbuf.at[k * 2 + r], peer, keep=True))
+        wbuf[0] = wrow[0]
+        return copies
+
+    for load in token_loads[:2]:
+        load.wait()
     for load in (mixer_load, *loads, pool_load):
         load.start()
 
     def scale_quarter(quarter):
         for j in range(width // 128):
             cols = columns(quarter, 128, j * 128)
-            value = tokens_in[:, cols].astype(jnp.float32) * row_factor[...]
-            scaled[:, j * 128 : (j + 1) * 128] = (value * moe_gain_ref[:, cols]).astype(
-                jnp.bfloat16
-            )
-
-    flushed = [0]
-
-    def flush(recent):
-        last = max(flushed[0], len(started) - recent)
-        for copy in started[flushed[0] : last]:
-            copy.wait_send()
-        flushed[0] = last
+            value = tokens_in[:, cols].astype(jnp.float32) * moe_gain_ref[:, cols]
+            scaled[:, j * 128 : (j + 1) * 128] = value.astype(jnp.bfloat16)
 
     def own_rows(quarter):
         return [xbuf.at[quarter, h, mine] for h in range(parts)]
@@ -242,12 +278,13 @@
 
     def depart(k, across):
         g = k // parts
-        index = g if g > 1 else across
+        index = g + 2 if across else g - 1
         rows = slice(k % parts * part, (k % parts + 1) * part)
         zcopies[k, across] = go(
             outgoing.at[index, rows],
             xbuf.at[xq if across else tp, k, mine],
             dev(planes[g], y, x, c),
+            keep=True,
         )
 
     def share(name, k, quarter, source, target, peer, start=0, stop=None):
@@ -258,20 +295,17 @@
                 xbuf.at[quarter, k, source, cols], xbuf.at[quarter, k, target, cols], peer
             )
 
-    pick_rows(tp, (1, 2, 3, 0), [outgoing.at[0], outgoing.at[2], outgoing.at[3]] + own_rows(tp))
+    pick_rows(tp, (1, 2, 3, 0), [outgoing.at[i] for i in range(3)] + own_rows(tp))
     pl.semaphore_wait(barrier, len(peers))
-    wcopies = []
-    for k in range(GROUPS):
-        for r in range(2):
-            if k or r:
-                peer = dev(planes[k], lax.rem(y + r, 2), x, c)
-                wcopies.append(go(wrow.at[k], wbuf.at[k * 2 + r], peer))
     depart(5, 0)
+    for k in range(parts):
+        share("y", k, tp, mine, theirs, y_peer)
+    for load in token_loads[2:]:
+        load.wait()
+    wcopies = send_lines()
+    pick_rows(xq, (1, 0), [outgoing.at[3]] + own_rows(xq))
     depart(2, 0)
     depart(3, 0)
-    for k in range(parts):
-        share("y", k, tp, mine, theirs, y_peer)
-    pick_rows(xq, (1, 0), [outgoing.at[1]] + own_rows(xq))
     depart(2, 1)
     depart(6, 0)
     depart(4, 0)
@@ -284,18 +318,18 @@
         down_copies.append(
             go(down_hbm.at[:, columns(xx * 2 + 1 - c)], w_down.at[xx, down_rows, :], core_peer)
         )
-    for quarter in (x * 2 + 1 - c, (1 - x) * 2 + 1 - c):
+    for quarter in quarters[2:]:
         pick_rows(quarter, (0,), own_rows(quarter))
 
     def arrive(k):
         zcopies[k, 0].wait_recv()
         share("y", k, tp, mine, theirs, y_peer)
-        if k // parts > 1:
+        if (k, 1) not in zcopies:
             share("x", k, tp, mine, mine, x_peer)
         share("c", k, tp, mine, mine, core_peer)
 
     def across(k):
-        if k // parts == 1:
+        if (k, 1) in zcopies:
             zcopies[k, 1].wait_recv()
         else:
             piece["x", k].wait_recv()
@@ -325,7 +359,9 @@
             copy.wait_recv()
         for source in range(wbuf.shape[0]):
             line = jnp.where(y == 0, wbuf[source, 0:1, :], wbuf[source, 1:2, :])
-            wcol[source * cap : (source + 1) * cap, :] = jnp.broadcast_to(line, (128, 128)).T[:cap]
+            at = slice(source * cap, (source + 1) * cap)
+            wcol[at, :] = jnp.broadcast_to(line, (128, 128)).T[:cap]
+            fcol[at, :] = jnp.broadcast_to(wbuf[source, 2:3, :], (128, 128)).T[:cap]
         for load in loads:
             load.wait()
         for copy in down_copies:
@@ -344,11 +380,14 @@
                 rows, w_up[q * width : (q + 1) * width, :], preferred_element_type=jnp.float32
             )
         first = k // parts * 2 * cap + k % parts * part
-        scale = jnp.concatenate(
-            [wcol[first : first + part, :], wcol[first + cap : first + cap + part, :]], axis=0
-        )
-        scale = jnp.concatenate([scale] * (units // scale.shape[1]), axis=1)
-        value = (gate / (1.0 + jnp.exp(-gate))) * upper * scale
+
+        def spread(table):
+            lines = [table[first : first + part, :], table[first + cap : first + cap + part, :]]
+            return jnp.concatenate([jnp.concatenate(lines, axis=0)] * (units // 128), axis=1)
+
+        factor = spread(fcol)
+        gate, upper = gate * factor, upper * factor
+        value = (gate / (1.0 + jnp.exp(-gate))) * upper * spread(wcol)
         hidden[c, k] = value.astype(jnp.bfloat16)
         hidden_away[k] = go(hidden.at[c, k], hidden.at[c, k], core_peer)
 
@@ -397,7 +436,8 @@
             else:
                 sums[k, x, mine, cols] = total.astype(jnp.bfloat16)
         if k >= parts:
-            home[k] = go(sums.at[k, x, mine, :], fin.at[k], dev(planes[k // parts], y, x, c))
+            peer = dev(planes[k // parts], y, x, c)
+            home[k] = go(sums.at[k, x, mine, :], fin.at[k], peer, keep=True)
 
     settled = []
 
@@ -430,6 +470,8 @@
 
     def square_sums():
         mixer_load.wait()
+        for load in small_loads[3:]:
+            load.wait()
 
         @pl.loop(0, tiles)
         def _(i):
@@ -460,7 +502,12 @@
 
         following = lax.rem(ep + 1, 2 * GROUPS)
         mixer_copies.append(
-            go(normed.at[rows : rows + reach, :], normed.at[0:reach, :], (following, tp))
+            go(
+                normed.at[rows : rows + reach, :],
+                normed.at[0:reach, :],
+                (following, tp),
+                keep=True,
+            )
         )
 
     def halo():
@@ -497,9 +544,9 @@
     arrive(2)
     diagonal(0)
     relay(1)
-    weights_ready()
     arrive(5)
     relay(2)
+    weights_ready()
     expand(0)
     relay(5)
     arrive(3)
@@ -535,7 +582,6 @@
     diagonal(6)
     expand(4)
     pool(0, 1)
-    flush(24)
     homeward(0)
     expand(1)
     project(4)
@@ -549,15 +595,12 @@
     second_x(4)
     diagonal(3)
     pool(1, 2)
-    flush(24)
     second_y(4)
     project(6)
     expand(3)
     homeward(5)
     pool(2, 3)
-    flush(24)
     pool(3, 4)
-    flush(24)
     homeward(4)
     project(3)
     second_y(7)
@@ -568,36 +611,25 @@
     second_y(3)
     project(1)
     pool(4, 5)
-    flush(24)
     homeward(6)
     pool(5, 6)
-    flush(24)
-    flush(16)
     settle(0)
     homeward(7)
     pool(6, 7)
-    flush(24)
-    flush(16)
     settle(4)
     homeward(3)
-    flush(16)
     settle(2)
     second_x(1)
     second_y(1)
     pool(7, 8)
-    flush(24)
-    flush(16)
     settle(6)
     homeward(1)
-    flush(16)
     settle(5)
-    flush(16)
     settle(1)
-    flush(16)
     settle(3)
-    flush(16)
     settle(7)
-    flush(0)
+    for index in kept + ring[-spare:]:
+        started[index].wait_send()
 
 
 def deliver(moe_in_ref, mixed_in_ref, moe_hbm, mixer_hbm, sem):
@@ -637,29 +669,36 @@
     hbm = pl.BlockSpec(memory_space=pl.ANY)
     dma = pltpu.SemaphoreType.DMA
     rows, channels = mixer_in.shape
-    copies = 150
+    spare = 32
+    copies, kept = 117, 22
     parts = 2
     chunks, part = GROUPS * parts, cap // parts
     moe_shape = (tokens, width)
     mixer_shape = (rows, channels)
     moe_out, mixed = pl.pallas_call(
-        functools.partial(expert_kernel, cap, parts),
+        functools.partial(expert_kernel, cap, parts, spare),
         out_shape=(
             pltpu.VMEM(moe_shape, jnp.bfloat16),
             pltpu.VMEM(mixer_shape, jnp.bfloat16),
         ),
-        in_specs=[hbm, vmem, vmem, vmem, hbm, hbm, hbm, hbm, vmem, hbm, vmem],
+        in_specs=[hbm] * 11,
         out_specs=(vmem, vmem),
         scratch_shapes=[
+            pltpu.VMEM((1, model), jnp.float32),
+            pltpu.VMEM(route_expert.shape[::-1], jnp.int32),
+            pltpu.VMEM(route_weight.shape[::-1], jnp.float32),
+            pltpu.VMEM((1, channels), jnp.float32),
+            pltpu.VMEM((1, channels), jnp.float32),
             pltpu.VMEM((tokens, model), jnp.bfloat16),
             pltpu.VMEM((tokens, 128), jnp.float32),
             pltpu.VMEM((tokens, width), jnp.bfloat16),
-            pltpu.VMEM((GROUPS, cap, width), jnp.bfloat16),
+            pltpu.VMEM((6, cap, width), jnp.bfloat16),
             pltpu.VMEM((tokens, 128), jnp.float32),
             pltpu.VMEM((tokens, width), jnp.float32),
             pltpu.VMEM((n_tp, chunks, 2 * part, width), jnp.bfloat16),
             pltpu.VMEM((GROUPS, 8, 128), jnp.float32),
             pltpu.VMEM((n_ep, 8, 128), jnp.float32),
+            pltpu.VMEM((n_ep * cap, 128), jnp.float32),
             pltpu.VMEM((n_ep * cap, 128), jnp.float32),
             pltpu.VMEM((model, units), jnp.bfloat16),
             pltpu.VMEM((model, units), jnp.bfloat16),
@@ -670,8 +709,8 @@
             pltpu.VMEM((chunks, 2, part, width // 2), jnp.bfloat16),
             pltpu.VMEM((chunks, 2, part, width // 2), jnp.bfloat16),
             pltpu.VMEM((chunks, part, width), jnp.bfloat16),
-            dma((14,)),
-            dma((copies,)),
+            dma((21,)),
+            dma((spare + kept,)),
             dma((copies,)),
             pltpu.VMEM((rows, channels), jnp.bfloat16),
             pltpu.VMEM(pool_weight.shape[1:], jnp.bfloat16),

time: 71.5 us -> 68.5 us (0.958)
  Pallas kernels: 70.4 us -> 67.5 us
    pallas_call x1, Pallas kernels: 68.8 us -> 65.8 us  [paired_step(): pl.pallas_call(functools.partial(expert_kernel, cap, parts, spare), out_s...]
where the time goes in v2:
time: 68.5 us; the launch traced here: 68.3 us
  Pallas kernels  67.5 us (99%)
  between operations  0.8 us (1%)
    pallas_call x1, Pallas kernels, paired_step(): pl.pallas_call(functools.partial(expert_kernel, cap, parts, spare), out_s...  65.8 us
    pallas_call x1, Pallas kernels, paired_step(): pl.pallas_call(deliver, out_shape=(jax.ShapeDtypeStruct(moe_shape, jnp.bf...  1.65 us

profile of v2, /device:TPU:0, one launch (start us, length us, event | category | flops | bytes accessed | tf_op | source)
XLA Modules:
  0.0 68.3 jit_solution(9980080094778892073)
XLA Ops:
  0.6 65.8 %shard_map.122 = (bf16[256,1024]{1,0:T(8,128)(2,1)S(1)}, bf16[1024,1024]{1,0:T(8,128)(2,1)S(1)}) custom-call(bf16[256,4096]{1,0:T(8,128)(2,1)} %moe_hbm.1, f32[1,4096]{1,0:T(1,128)} %bitcast.13, s32[2,256]{1,0:T(2,128)} %bitcast.16, f32[2,256]{1,0:T(2,128)} %bitcast.17, bf16[4096,256]{1,0:T(8,128)(2,1)} %bitcast.9, bf16[4096,256]{1,0:T(8,128)(2,1)} %bitcast.10, ...), custom_call_target="tpu_custom_call" | custom-call | tf_op jit(solution)/shard_map/pallas_call | solution.py:678
  66.5 1.6 %shard_map.123 = (bf16[256,1024]{1,0:T(8,128)(2,1)}, bf16[1024,1024]{1,0:T(8,128)(2,1)}) custom-call(bf16[256,1024]{1,0:T(8,128)(2,1)S(1)} %get-tuple-element.6.moe_in_ref, bf16[1024,1024]{1,0:T(8,128)(2,1)S(1)} %get-tuple-element.7.mixed_in_ref), custom_call_target="tpu_custom_call" | custom-call | tf_op jit(solution)/shard_map/pallas_call | solution.py:738

commit v3 on v2

--- a/solution.py
+++ b/solution.py
@@ -157,6 +157,28 @@
 
     ring = []
     kept = []
+    arrivals = [0]
+    clock = [0]
+    exchanged = {id(core_peer): [], id(x_peer): [], id(y_peer): []}
+
+    class Copy:
+        def __init__(self, copy):
+            self.copy, self.sent, self.waited = copy, clock[0], None
+            self.wait_send = copy.wait_send
+
+        def wait_recv(self):
+            self.copy.wait_recv()
+            clock[0] += 1
+            self.waited = clock[0]
+
+    def receiver(past):
+        heard = max((copy.sent for copy in past if copy.waited is not None), default=0)
+        latest = {copy.index: copy for copy in past}
+        for index, copy in latest.items():
+            if copy.waited is not None and copy.waited < heard:
+                return index
+        arrivals[0] += 1
+        return arrivals[0] - 1
 
     def go(src, dst, peer, keep=False):
         index = len(started)
@@ -168,17 +190,22 @@
             if len(ring) >= spare:
                 started[ring[-spare]].wait_send()
             ring.append(index)
+        past = exchanged.get(id(peer), [])
+        receive = receiver(past)
         copy = pltpu.make_async_remote_copy(
             src_ref=src,
             dst_ref=dst,
             send_sem=send_sem.at[send],
-            recv_sem=recv_sem.at[index],
+            recv_sem=recv_sem.at[receive],
             device_id=peer,
             device_id_type=MESH,
         )
         copy.start()
-        started.append(copy)
-        return copy
+        clock[0] += 1
+        started.append(Copy(copy))
+        started[-1].index = receive
+        past.append(started[-1])
+        return started[-1]
 
     for load in small_loads[:3]:
         load.wait()
@@ -240,7 +267,7 @@
             for r in range(2):
                 if k or r:
                     peer = dev(planes[k], lax.rem(y + r, 2), x, c)
-                    copies.append(go(wrow.at[k], wbuf.at[k * 2 + r], peer, keep=True))
+                    copies.append(go(wrow.at[k], wbuf.at[k * 2 + r], peer))
         wbuf[0] = wrow[0]
         return copies
 
@@ -437,7 +464,7 @@
                 sums[k, x, mine, cols] = total.astype(jnp.bfloat16)
         if k >= parts:
             peer = dev(planes[k // parts], y, x, c)
-            home[k] = go(sums.at[k, x, mine, :], fin.at[k], peer, keep=True)
+            home[k] = go(sums.at[k, x, mine, :], fin.at[k], peer)
 
     settled = []
 
@@ -506,7 +533,6 @@
                 normed.at[rows : rows + reach, :],
                 normed.at[0:reach, :],
                 (following, tp),
-                keep=True,
             )
         )
 
@@ -578,9 +604,9 @@
     second_y(0)
     second_y(2)
     project(5)
-    halo()
     diagonal(6)
     expand(4)
+    halo()
     pool(0, 1)
     homeward(0)
     expand(1)
@@ -670,7 +696,7 @@
     dma = pltpu.SemaphoreType.DMA
     rows, channels = mixer_in.shape
     spare = 32
-    copies, kept = 117, 22
+    copies, kept = 67, 8
     parts = 2
     chunks, part = GROUPS * parts, cap // parts
     moe_shape = (tokens, width)

time: 68.5 us -> 67.9 us (level)
  no operation moved by 1% of the time
where the time goes in v3:
time: 67.9 us; the launch traced here: 67.7 us
  Pallas kernels  66.9 us (99%)
  between operations  0.8 us (1%)
    pallas_call x1, Pallas kernels, paired_step(): pl.pallas_call(functools.partial(expert_kernel, cap, parts, spare), out_s...  65.2 us
    pallas_call x1, Pallas kernels, paired_step(): pl.pallas_call(deliver, out_shape=(jax.ShapeDtypeStruct(moe_shape, jnp.bf...  1.65 us

profile of v3, /device:TPU:0, one launch (start us, length us, event | category | flops | bytes accessed | tf_op | source)
XLA Modules:
  0.0 67.7 jit_solution(13953676863159788375)
XLA Ops:
  0.6 65.2 %shard_map.122 = (bf16[256,1024]{1,0:T(8,128)(2,1)S(1)}, bf16[1024,1024]{1,0:T(8,128)(2,1)S(1)}) custom-call(bf16[256,4096]{1,0:T(8,128)(2,1)} %moe_hbm.1, f32[1,4096]{1,0:T(1,128)} %bitcast.13, s32[2,256]{1,0:T(2,128)} %bitcast.16, f32[2,256]{1,0:T(2,128)} %bitcast.17, bf16[4096,256]{1,0:T(8,128)(2,1)} %bitcast.9, bf16[4096,256]{1,0:T(8,128)(2,1)} %bitcast.10, ...), custom_call_target="tpu_custom_call" | custom-call | tf_op jit(solution)/shard_map/pallas_call | solution.py:704
  65.9 1.6 %shard_map.123 = (bf16[256,1024]{1,0:T(8,128)(2,1)}, bf16[1024,1024]{1,0:T(8,128)(2,1)}) custom-call(bf16[256,1024]{1,0:T(8,128)(2,1)S(1)} %get-tuple-element.6.moe_in_ref, bf16[1024,1024]{1,0:T(8,128)(2,1)S(1)} %get-tuple-element.7.mixed_in_ref), custom_call_target="tpu_custom_call" | custom-call | tf_op jit(solution)/shard_map/pallas_call | solution.py:764
